TPU v7x, 32 devices: a whole 2x2x4 slice. The times are simulated.
32 devices in a mesh: fs: 8 (over z, x), tp: 4 (over y, core).
Axes of the slice: x: 2, y: 2, z: 4, core: 2. Of those that a mesh axis runs over, the one named last changes fastest.
Arguments:
- inputs: bfloat16 [8192, 4096], P('fs'), may hold values from -8 to 8
- value_cot: bfloat16 [8192, 2048], P('fs', 'tp'), may hold values from -0.015625 to 0.015625
- gate_cot: bfloat16 [8192, 2048], P('fs', 'tp'), may hold values from -0.015625 to 0.015625
- out_cot: bfloat16 [8192, 4096], P('fs'), may hold values from -0.0234375 to 0.0234375
- conv_output: bfloat16 [8192, 2048], P('fs', 'tp'), may hold values from -6 to 6
- factors: bfloat16 [3, 4096, 256], P(None, 'fs'), may hold values from -0.375 to 0.375
- value_weight: float32 [4096, 2048], P('fs', 'tp'), may hold values from -0.09375 to 0.09375
- gate_weight: float32 [4096, 2048], P('fs', 'tp'), may hold values from -0.09375 to 0.09375
- out_weight: float32 [2048, 4096], P('tp', 'fs'), may hold values from -0.125 to 0.125
- first_moment: float32 [3, 256, 2048], P(None, 'fs', 'tp'), may hold values from -7.2 to 7.2
- second_moment: float32 [3, 256, 2048], P(None, 'fs', 'tp'), may hold values from 0.005 to 0.05
Outputs:
- new_first: float32 [3, 256, 2048], P(None, 'fs', 'tp')
- new_second: float32 [3, 256, 2048], P(None, 'fs', 'tp')
- value_update: float32 [4096, 2048], P('fs', 'tp')
- gate_update: float32 [4096, 2048], P('fs', 'tp')
- out_update: float32 [2048, 4096], P('tp', 'fs')
- value_copy: bfloat16 [4096, 2048], P(None, 'tp')
- gate_copy: bfloat16 [4096, 2048], P(None, 'tp')
- out_copy: bfloat16 [2048, 4096], P('tp')
All inputs are finite; a program needn't handle non-finite values.
Results may differ from a plain program's by a relative error of at most 0.001.
Values may be sent and summed in bfloat16 or wider, within the bound.
A program may use at most 128 MiB of HBM per device.

v0:
```python
import jax
import jax.numpy as jnp
from jax import lax
from jax.sharding import PartitionSpec as P

C = 2048
RANK = 256


FIRST_DECAY = 0.9
SECOND_DECAY = 0.95
DIVISOR_EPS = 1e-08
SQUARE_EPS = 1e-06
LEARN_RATE = 0.01


def high_low(values):
    upper = lax.optimization_barrier(values.astype(jnp.bfloat16))
    lower = (values - upper.astype(jnp.float32)).astype(jnp.bfloat16)
    return (upper, lower)


def split_product(left, right, transposed):
    upper, lower = high_low(right)
    operand = left.T if transposed else left
    first_part = jnp.dot(operand, upper, preferred_element_type=jnp.float32)
    return first_part + jnp.dot(operand, lower, preferred_element_type=jnp.float32)


def shards(
    inputs,
    value_cot,
    gate_cot,
    out_cot,
    conv_output,
    factors,
    value_weight,
    gate_weight,
    out_weight,
    first_moment,
    second_moment,
):
    col_width = value_cot.shape[1]
    rows_small = first_moment.shape[1]
    pieces = lax.all_gather(factors, "fs", axis=1, tiled=True)
    summed = jnp.stack(
        [
            jnp.dot(inputs, pieces[0], preferred_element_type=jnp.float32),
            jnp.dot(inputs, pieces[1], preferred_element_type=jnp.float32),
            jnp.dot(out_cot, pieces[2], preferred_element_type=jnp.float32),
        ]
    )
    partial_value = jnp.concatenate(
        [
            split_product(value_cot, summed[0], True).T,
            split_product(gate_cot, summed[1], True).T,
            split_product(conv_output, summed[2], True).T,
        ],
        axis=1,
    )
    projected = lax.psum_scatter(partial_value, "fs", scatter_dimension=0, tiled=True)
    first_cols = jnp.transpose(first_moment, (1, 0, 2)).reshape(rows_small, 3 * col_width)
    second_cols = jnp.transpose(second_moment, (1, 0, 2)).reshape(rows_small, 3 * col_width)
    new_first = FIRST_DECAY * first_cols + (1.0 - FIRST_DECAY) * projected
    new_second = SECOND_DECAY * second_cols + (1.0 - SECOND_DECAY) * projected * projected
    direction = new_first / (jnp.sqrt(new_second) + DIVISOR_EPS)
    collected = lax.all_gather(direction, "fs", axis=0, tiled=True)
    sum_squares = lax.psum(jnp.sum(direction * direction), ("fs", "tp"))
    norm_scale = lax.rsqrt(sum_squares / (3 * RANK * C) + SQUARE_EPS)
    updates = [
        norm_scale
        * split_product(
            factors[index], collected[:, index * col_width : (index + 1) * col_width], False
        )
        for index in range(3)
    ]
    out_update = updates[2].T
    copies = (
        lax.all_gather(
            (value_weight - LEARN_RATE * updates[0]).astype(jnp.bfloat16), "fs", axis=0, tiled=True
        ),
        lax.all_gather(
            (gate_weight - LEARN_RATE * updates[1]).astype(jnp.bfloat16), "fs", axis=0, tiled=True
        ),
        lax.all_gather(
            (out_weight - LEARN_RATE * out_update).astype(jnp.bfloat16), "fs", axis=1, tiled=True
        ),
    )
    first_out = jnp.transpose(new_first.reshape(rows_small, 3, col_width), (1, 0, 2))
    second_out = jnp.transpose(new_second.reshape(rows_small, 3, col_width), (1, 0, 2))
    return (
        first_out,
        second_out,
        updates[0],
        updates[1],
        out_update,
        copies[0],
        copies[1],
        copies[2],
    )


def solution(mesh):
    placed = (
        P("fs", None),
        P("fs", "tp"),
        P("fs", "tp"),
        P("fs", None),
        P("fs", "tp"),
        P(None, "fs", None),
        P("fs", "tp"),
        P("fs", "tp"),
        P("tp", "fs"),
        P(None, "fs", "tp"),
        P(None, "fs", "tp"),
    )
    return jax.shard_map(
        shards,
        mesh=mesh,
        in_specs=placed,
        out_specs=(
            P(None, "fs", "tp"),
            P(None, "fs", "tp"),
            P("fs", "tp"),
            P("fs", "tp"),
            P("tp", "fs"),
            P(None, "tp"),
            P(None, "tp"),
            P("tp", None),
        ),
        check_vma=False,
    )
```

profile of v0, /device:TPU:0, one launch (start us, length us, event | category | flops | bytes accessed | tf_op | source)
XLA Modules:
  0.0 483.6 jit_solution(10768886611922828320)
XLA Ops:
  7.2 0.7 all-gather.6.cloned.1.call-update
  8.0 103.7 %all-gather.6.cloned.1.call-done = bf16[3,4096,256]{2,1,0:T(8,128)(2,1)} async-done(((bf16[3,512,256]{2,1,0:T(8,128)(2,1)}), bf16[3,4096,256]{2,1,0:T(8,128)(2,1)}) %all-gather.6.cloned.1.call-update) | async-done | bytes 6291472 | tf_op jit(solution)/shard_map/all_gather | solution.py:45
  111.6 6.5 %fusion.26 = (bf16[1024,256]{1,0:T(8,128)(2,1)S(1)}, f32[1024,256]{1,0:T(8,128)S(1)}) fusion(bf16[1024,4096]{1,0:T(8,128)(2,1)} %param.14, bf16[3,4096,256]{2,1,0:T(8,128)(2,1)} %all-gather.6.cloned.1.call-done), kind=kOutput, calls=%fused_computation.53 | convolution fusion | flops 2147745792 | bytes 12058624 | tf_op jit(solution)/shard_map/dot_general | solution.py:50
  118.1 5.9 %fusion.28 = (bf16[1024,256]{1,0:T(8,128)(2,1)S(1)}, f32[1024,256]{1,0:T(8,128)S(1)}) fusion(bf16[1024,4096]{1,0:T(8,128)(2,1)} %param.11, bf16[3,4096,256]{2,1,0:T(8,128)(2,1)S(1)} %copy-done.10), kind=kOutput, calls=%fused_computation.55 | convolution fusion | flops 2147745792 | bytes 12058624 | tf_op jit(solution)/shard_map/dot_general | solution.py:48
  124.0 2.3 fusion.27
  126.4 0.4 fusion.31
  126.8 0.5 convolution_add_fusion.3
  127.6 0.4 fusion.30
  128.0 0.5 convolution_add_fusion.4
  128.5 0.5 fusion.29
  129.0 0.5 convolution_add_fusion.5
  129.5 1.3 pad_maximum_fusion
  131.0 63.7 %reduce-scatter.2.cloned.1.call-done = f32[32,1536]{1,0:T(8,128)} async-done(((f32[256,1536]{1,0:T(8,128)}), f32[32,1536]{1,0:T(8,128)}) %reduce-scatter.2.cloned.1.call-update) | async-done | bytes 196624 | tf_op jit(solution)/shard_map/reduce_scatter | solution.py:61
  194.6 2.4 multiply_reduce_fusion
  197.1 40.8 %psum.7 = f32[]{:T(128)} all-reduce(f32[]{:T(128)} %get-tuple-element.24), channel_id=1, replica_groups=mesh['fs'=8,'tp'=4] {'fs','tp'}, use_global_device_ids=true, to_apply=%region_2.0 | all-reduce | flops 1 | bytes 8 | tf_op jit(solution)/shard_map/psum | solution.py:68
  238.5 2.0 all-gather.8.cloned.1.call-done
  240.5 1.5 fusion.25
  242.3 2.5 subtract_convert_fusion.1
  244.9 1.6 copy.44
  246.7 2.2 subtract_convert_fusion
  249.2 2.6 copy.42
  252.1 2.6 subtract_convert_fusion.2
  254.9 0.7 copy.46
  255.8 0.7 copy.45
  256.5 1.3 copy.48
  257.8 1.3 copy.47
  259.2 57.1 %all-gather.12.cloned.1.call-done = bf16[4096,512]{1,0:T(8,128)(2,1)} async-done(((bf16[512,512]{1,0:T(8,128)(2,1)}), bf16[4096,512]{1,0:T(8,128)(2,1)}) %all-gather.12.cloned.1.call-update) | async-done | bytes 4194320 | tf_op jit(solution)/shard_map/all_gather | solution.py:82
  316.2 73.9 %all-gather.14.cloned.1.call-done = bf16[512,4096]{0,1:T(8,128)(2,1)} async-done(((bf16[512,512]{0,1:T(8,128)(2,1)}), bf16[512,4096]{0,1:T(8,128)(2,1)}) %all-gather.14.cloned.1.call-update) | async-done | bytes 4194320 | tf_op jit(solution)/shard_map/all_gather | solution.py:85
  390.1 6.3 %copy.50 = bf16[512,4096]{1,0:T(8,128)(2,1)} copy(bf16[512,4096]{0,1:T(8,128)(2,1)} %all-gather.14.cloned.1.call-done) | data formatting | bytes 8388608
  396.4 69.4 %all-gather.10.cloned.1.call-done = bf16[4096,512]{0,1:T(8,128)(2,1)} async-done(((bf16[512,512]{0,1:T(8,128)(2,1)}), bf16[4096,512]{0,1:T(8,128)(2,1)}) %all-gather.10.cloned.1.call-update) | async-done | bytes 4194320 | tf_op jit(solution)/shard_map/all_gather | solution.py:79
  465.8 6.4 %copy.49 = bf16[4096,512]{1,0:T(8,128)(2,1)} copy(bf16[4096,512]{0,1:T(8,128)(2,1)} %all-gather.10.cloned.1.call-done) | data formatting | bytes 8388608
  472.2 4.6 copy.58
  (47 shorter events, 2.1 us)
Async XLA Ops:
  7.2 119.2 %copy-start = (bf16[1024,512]{1,0:T(8,128)(2,1)S(1)}, bf16[1024,512]{1,0:T(8,128)(2,1)}, u32[]{:S(2)}) copy-start(bf16[1024,512]{1,0:T(8,128)(2,1)} %param.15) | copy-start | bytes 3145732
  7.2 104.4 %all-gather.6.cloned.1.call-start = ((), (), s32[]{:S(2)}) async-start(), calls=%async_computation.1 | async-start | bytes 7077888 | tf_op jit(solution)/shard_map/all_gather | solution.py:45
  7.9 186.7 %reduce-scatter.2.cloned.1.call-start = ((), (), s32[]{:S(2)}) async-start(), calls=%async_computation.2 | async-start | bytes 1769472 | tf_op jit(solution)/shard_map/reduce_scatter | solution.py:61
  111.6 6.5 %copy-start.10 = (bf16[3,4096,256]{2,1,0:T(8,128)(2,1)S(1)}, bf16[3,4096,256]{2,1,0:T(8,128)(2,1)}, u32[]{:S(2)}) copy-start(bf16[3,4096,256]{2,1,0:T(8,128)(2,1)} %all-gather.6.cloned.1.call-done) | copy-start | bytes 18874372
  111.6 12.4 %slice-start = ((s8[8388608]{0:T(1024)(128)(4,1)}), s8[4194304]{0:T(1024)(128)(4,1)S(1)}, s32[]{:S(2)}) async-start(s8[8388608]{0:T(1024)(128)(4,1)} %bitcast.69), calls=%async_computation.7 | async-start | bytes 8388608
  118.1 5.9 %slice-start.1 = ((s8[8388608]{0:T(1024)(128)(4,1)}), s8[4194304]{0:T(1024)(128)(4,1)S(1)}, s32[]{:S(2)}) async-start(s8[8388608]{0:T(1024)(128)(4,1)} %bitcast.69), calls=%async_computation.8 | async-start | bytes 8388608
  126.4 1.2 copy-start.3
  126.8 1.7 copy-start.4
  129.0 1.8 copy-start.8
  129.0 1.9 copy-start.9
  129.5 112.5 %copy-start.2 = (bf16[3,512,256]{2,1,0:T(8,128)(2,1)S(1)}, bf16[3,512,256]{2,1,0:T(8,128)(2,1)}, u32[]{:S(2)}) copy-start(bf16[3,512,256]{2,1,0:T(8,128)(2,1)} %param.16) | copy-start | bytes 2359300
  130.8 111.5 %copy-start.5 = (f32[512,512]{1,0:T(8,128)S(1)}, f32[512,512]{1,0:T(8,128)}, u32[]{:S(2)}) copy-start(f32[512,512]{1,0:T(8,128)} %param.18) | copy-start | bytes 3145732
  130.8 109.7 %all-gather.8.cloned.1.call-start = ((), (), s32[]{:S(2)}) async-start(), calls=%async_computation.3 | async-start | bytes 1769472 | tf_op jit(solution)/shard_map/all_gather | solution.py:67
  197.0 119.2 %all-gather.12.cloned.1.call-start = ((), (), s32[]{:S(2)}) async-start(), calls=%async_computation.5 | async-start | bytes 4718592 | tf_op jit(solution)/shard_map/all_gather | solution.py:82
  244.8 145.3 %all-gather.14.cloned.1.call-start = ((), (), s32[]{:S(2)}) async-start(), calls=%async_computation.6 | async-start | bytes 4718592 | tf_op jit(solution)/shard_map/all_gather | solution.py:85
  248.9 5.8 %copy-start.7 = (f32[32,1536]{1,0:T(8,128)S(1)}, f32[32,1536]{1,0:T(8,128)}, u32[]{:S(2)}) copy-start(f32[32,1536]{1,0:T(8,128)} %get-tuple-element.26) | copy-start | bytes 589828
  249.0 216.8 %all-gather.10.cloned.1.call-start = ((), (), s32[]{:S(2)}) async-start(), calls=%async_computation.4 | async-start | bytes 4718592 | tf_op jit(solution)/shard_map/all_gather | solution.py:79
  251.7 3.9 copy-start.6
  472.2 4.6 copy-start.1
Sparse Core Ops, SparseCore 0:
  10.2 101.4 all-gather.5
  130.9 63.6 reduce-scatter.1
  197.4 43.1 all-gather.7
  245.0 71.2 all-gather.11
  318.8 71.3 all-gather.13
  392.6 73.1 all-gather.9
where the time goes:
time: 484 us
  waiting for transfers between devices  370 us (76%)
  blocking collectives  40.8 us (8%)
  local copies, waits for them, and re-layouts  27.6 us (6%)
  matrix products  25.7 us (5%)
  between operations  15.1 us (3%)
    all_gather x1, waiting for transfers between devices, shards(): pieces = lax.all_gather(factors, 'fs', axis=1, tiled=True)  104 us
    all_gather x1, waiting for transfers between devices, shards(): lax.all_gather((out_weight - LEARN_RATE * out_update).astype(jnp.bfloat16...  73.9 us
    all_gather x1, waiting for transfers between devices, shards(): lax.all_gather((value_weight - LEARN_RATE * updates[0]).astype(jnp.bfloat...  69.4 us
    reduce_scatter x1, waiting for transfers between devices, shards(): lax.psum_scatter(partial_value, 'fs', scatter_dimension=0, tiled=True)  63.7 us
    all_gather x1, waiting for transfers between devices, shards(): lax.all_gather((gate_weight - LEARN_RATE * updates[1]).astype(jnp.bfloat1...  57.1 us
    psum x1, blocking collectives, shards(): sum_squares = lax.psum(jnp.sum(direction * direction), ('fs', 'tp'))  40.8 us
    unnamed x35, local copies, waits for them, and re-layouts  25.8 us
  transfers between devices with their start and end apart: 6, of which 6 were waited for; matrix products, arithmetic and copies ran while one was open for 4% of the time, Pallas kernels for 0%

commit v1 on v0

v1 whole, which is shorter than its diff:
```python
import functools

import jax
import jax.numpy as jnp
from jax import lax
from jax.experimental import pallas as pl
from jax.experimental.pallas import tpu as pltpu
from jax.sharding import PartitionSpec as P

FIRST_DECAY = 0.9
SECOND_DECAY = 0.95
DIVISOR_EPS = 1e-08
SQUARE_EPS = 1e-06
LEARN_RATE = 0.01
MESH = pl.DeviceIdType.MESH
F32 = jnp.float32
BF16 = jnp.bfloat16


def high_low(values):
    upper = values.astype(BF16)
    lower = (values - upper.astype(F32)).astype(BF16)
    return upper, lower


def others(coord, size, dist):
    if dist == 0:
        return [(coord, 0, None)]
    if size == 2:
        return [(1 - coord, None, None)]
    return [(coord - dist, -1, coord >= dist), (coord + dist, 1, coord + dist < size)]


def both(*preds):
    preds = [p for p in preds if p is not None]
    if not preds:
        return None
    return functools.reduce(jnp.logical_and, preds)


def run_if(pred, fn):
    if pred is None:
        fn()
    else:
        pl.when(pred)(fn)


def kernel(
    nz, nx, tp,
    x_hbm, oc_hbm, vc_hbm, gc_hbm, co_hbm, f_hbm, w0_hbm, w1_hbm, w2_hbm, m1_ref, m2_ref,
    nf_ref, ns_ref, u0_hbm, u1_hbm, u2_hbm, c0_hbm, c1_hbm, c2_hbm,
    x_v, oc_v, cots, fg, wts, acc, part, rx, rz, q, dg, dh, dl, upd, upd_t, own01, own2, ss,
    in_sem, loc_sem, f_recv, f_send, y_recv, y_send, p_recv, p_send,
    rx_recv, rx_send, rz_recv, rz_send, d_recv, d_send, s_recv, s_send, c_recv, c_send,
):
    me = lax.axis_index("fs")
    t = lax.axis_index("tp")
    z = lax.div(me, nx)
    x = lax.rem(me, nx)
    n = nz * nx
    core = lax.rem(t, 2)
    row = lax.rem(lax.div(t, 2), 2)
    mate = t + 1 - 2 * core
    beside = t + 2 - 4 * row
    block = f_hbm.shape[1]
    rank = f_hbm.shape[2]
    rows = m1_ref.shape[1]
    width = m1_ref.shape[2]
    tokens = x_hbm.shape[0]
    pending = []

    def remote(src, dst, ssem, rsem, where):
        copy = pltpu.make_async_remote_copy(
            src_ref=src, dst_ref=dst, send_sem=ssem, recv_sem=rsem,
            device_id=where, device_id_type=MESH,
        )
        return copy

    def send(src, dst, ssem, rsem, where, pred, outer):
        copy = remote(src, dst, ssem, rsem, where)
        pred = both(pred, outer)
        run_if(pred, copy.start)
        pending.append((pred, copy))

    def drain():
        for pred, copy in pending:
            run_if(pred, copy.wait_send)
        pending.clear()

    loads = [
        pltpu.make_async_copy(f_hbm, fg.at[me], in_sem.at[0]),
        pltpu.make_async_copy(x_hbm, x_v, in_sem.at[1]),
        pltpu.make_async_copy(oc_hbm, oc_v, in_sem.at[2]),
        pltpu.make_async_copy(vc_hbm, cots.at[0], in_sem.at[3]),
        pltpu.make_async_copy(gc_hbm, cots.at[1], in_sem.at[4]),
        pltpu.make_async_copy(co_hbm, cots.at[2], in_sem.at[5]),
        pltpu.make_async_copy(w0_hbm, wts[0], in_sem.at[6]),
        pltpu.make_async_copy(w1_hbm, wts[1], in_sem.at[7]),
        pltpu.make_async_copy(w2_hbm, wts[2], in_sem.at[8]),
    ]
    for load in loads:
        load.start()

    barrier = pltpu.get_barrier_semaphore()
    peers = [{"fs": lax.rem(z + k, nz) * nx + x} for k in range(1, nz)]
    peers += [{"fs": z * nx + lax.rem(x + k, nx)} for k in range(1, nx)]
    peers += [{"tp": lax.rem(t + k, tp)} for k in range(1, tp)]
    for peer in peers:
        pl.semaphore_signal(barrier, inc=1, device_id=peer, device_id_type=MESH)
    pl.semaphore_wait(barrier, len(peers))

    def stage_items(s, z_first):
        n1, n2 = (nz, nx) if z_first else (nx, nz)
        c1, c2 = (z, x) if z_first else (x, z)
        items = []
        for e in range(0, n2):
            d = s - e
            if d < 0 or d >= n1:
                continue
            for o1, s1, v1 in others(c1, n1, d):
                for o2, s2, v2 in others(c2, n2, e):
                    slot = o1 * nx + o2 if z_first else o2 * nx + o1
                    items.append((d, e, s1, s2, slot, both(v1, v2)))
        return items

    def forward(item, z_first, src, dst, ssem, rsem):
        d, e, s1, s2, slot, valid = item
        n1, n2 = (nz, nx) if z_first else (nx, nz)
        c1, c2 = (z, x) if z_first else (x, z)
        st1, st2 = (nx, 1) if z_first else (1, nx)
        if e == 0:
            if s1 in (-1, 0):
                send(src, dst, ssem(0), rsem, {"fs": me + st1}, c1 + 1 < n1, valid)
            if s1 in (1, 0):
                send(src, dst, ssem(1 if s1 == 0 else 0), rsem, {"fs": me - st1}, c1 > 0, valid)
        if s2 in (-1, 0):
            send(src, dst, ssem(2), rsem, {"fs": me + st2}, c2 + 1 < n2, valid)
        if s2 in (1, 0):
            send(src, dst, ssem(3 if s2 == 0 else 2), rsem, {"fs": me - st2}, c2 > 0, valid)

    def arrived(dst, sem, pred=None):
        run_if(pred, pltpu.make_async_copy(dst, dst, sem).wait)

    unit = block // 16
    half = core * (block // 2)
    fs_start = pl.multiple_of(half + row * 3 * unit, unit)
    y_send_start = pl.multiple_of(half + row * 5 * unit, unit)
    y_recv_start = pl.multiple_of(half + (1 - row) * 5 * unit, unit)
    mate_half = (1 - core) * (block // 2)
    mate_fs_start = pl.multiple_of(mate_half + row * 3 * unit, unit)
    mate_y_start = pl.multiple_of(mate_half + (1 - row) * 5 * unit, unit)

    def f_part(slot, start, units):
        return fg.at[slot, :, pl.ds(start, units * unit), :]

    def matmuls(slot, first):
        cols = pl.ds(pl.multiple_of(slot * block, block), block)
        tile = 256

        def body(i, carry):
            r = pl.ds(pl.multiple_of(i * tile, tile), tile)
            for k, src in enumerate((x_v, x_v, oc_v)):
                prod = jnp.dot(src[r, cols], fg[slot, k], preferred_element_type=F32)
                if first:
                    acc[k, r, :] = prod
                else:
                    acc[k, r, :] += prod
            return carry

        lax.fori_loop(0, tokens // tile, body, 0)

    n_stages = nz + nx - 1
    queued = {}
    for s in range(n_stages + 2):
        if s < n_stages:
            items = stage_items(s, True)
            queued[s] = items
            if s == 0:
                loads[0].wait()
            for item in items:
                d, e, s1, s2, slot, valid = item

                piece = f_part(slot, fs_start, 5)
                if s > 0:
                    arrived(piece, f_recv.at[slot], valid)
                forward(item, True, piece, piece, lambda i: f_send.at[slot, i], f_recv.at[slot])
                if s > 0:
                    ypiece = f_part(slot, y_send_start, 3)
                    send(ypiece, ypiece, y_send.at[slot], y_recv.at[slot], {"tp": beside}, None, valid)
                    send(piece, piece, p_send.at[slot, 0], p_recv.at[slot, 0], {"tp": mate}, None, valid)
        if s == 0:
            loads[1].wait()
            loads[2].wait()
            matmuls(me, True)
        if s - 1 >= 1 and s - 1 < n_stages:
            for item in queued[s - 1]:
                slot, valid = item[4], item[5]

                ypiece = f_part(slot, y_recv_start, 3)
                arrived(ypiece, y_recv.at[slot], valid)
                send(ypiece, ypiece, p_send.at[slot, 1], p_recv.at[slot, 1], {"tp": mate}, None, valid)
        if s - 2 >= 1:
            for item in queued[s - 2]:
                slot, valid = item[4], item[5]

                def use(slot=slot):
                    arrived(f_part(slot, mate_fs_start, 5), p_recv.at[slot, 0])
                    arrived(f_part(slot, mate_y_start, 3), p_recv.at[slot, 1])
                    matmuls(slot, False)

                run_if(valid, use)
    drain()

    for load in loads[3:6]:
        load.wait()
    dims = (((0,), (0,)), ((), ()))
    for k in range(3):
        upper, lower = high_low(acc[k])
        prod = lax.dot_general(upper, cots[k], dims, preferred_element_type=F32)
        prod = prod + lax.dot_general(lower, cots[k], dims, preferred_element_type=F32)
        part[:, k] = prod.reshape(n, rows, width)

    order = list(range(1, nz)) + [0]
    for k in order:
        oz = lax.rem(z + k, nz)
        for e in range(1, nx):
            ox = lax.rem(x + e, nx)
            send(
                part.at[oz * nx + ox], rx.at[e - 1, k], rx_send.at[e - 1, k], rx_recv.at[e - 1, k],
                {"fs": z * nx + ox}, None, None,
            )
    for k in order:
        oz = lax.rem(z + k, nz)
        value = part[oz * nx + x]
        for e in range(1, nx):
            arrived(rx.at[e - 1, k], rx_recv.at[e - 1, k])
            value = value + rx[e - 1, k]
        q[k] = value
        if k:
            send(q.at[k], rz.at[k - 1], rz_send.at[k - 1], rz_recv.at[k - 1], {"fs": oz * nx + x}, None, None)
    projected = q[0]
    for k in range(1, nz):
        arrived(rz.at[k - 1], rz_recv.at[k - 1])
        projected = projected + rz[k - 1]
    new_first = FIRST_DECAY * m1_ref[...] + (1.0 - FIRST_DECAY) * projected
    new_second = SECOND_DECAY * m2_ref[...] + (1.0 - SECOND_DECAY) * projected * projected
    nf_ref[...] = new_first
    ns_ref[...] = new_second
    dg[me] = new_first / (jnp.sqrt(new_second) + DIVISOR_EPS)

    for s in range(n_stages):
        for item in stage_items(s, True):
            slot, valid = item[4], item[5]
            piece = dg.at[slot]
            if s > 0:
                arrived(piece, d_recv.at[slot], valid)
            forward(item, True, piece, piece, lambda i: d_send.at[slot, i], d_recv.at[slot])

    total = jnp.zeros((1, width), F32)
    for i in range(n):
        for k in range(3):
            piece = dg[i, k]
            total = total + jnp.sum(piece * piece, axis=0, keepdims=True)
            upper, lower = high_low(piece)
            dh[k, i * rows:(i + 1) * rows, :] = upper
            dl[k, i * rows:(i + 1) * rows, :] = lower
    total = jnp.sum(total, axis=1, keepdims=True)
    ss[0] = jnp.broadcast_to(total, ss.shape[1:])
    for j in range(1, tp):
        send(ss.at[0], ss.at[j], s_send.at[j - 1], s_recv.at[j - 1], {"tp": lax.rem(t + j, tp)}, None, None)
    for load in loads[6:9]:
        load.wait()
    upd[0] = jnp.dot(fg[me, 0], dh[0], preferred_element_type=F32) + jnp.dot(
        fg[me, 0], dl[0], preferred_element_type=F32
    )
    upd[1] = jnp.dot(fg[me, 1], dh[1], preferred_element_type=F32) + jnp.dot(
        fg[me, 1], dl[1], preferred_element_type=F32
    )
    tdims = (((0,), (1,)), ((), ()))
    upd_t[...] = lax.dot_general(dh[2], fg[me, 2], tdims, preferred_element_type=F32) + lax.dot_general(
        dl[2], fg[me, 2], tdims, preferred_element_type=F32
    )
    sums = ss[0]
    for j in range(1, tp):
        arrived(ss.at[j], s_recv.at[j - 1])
        sums = sums + ss[j]
    scale = lax.rsqrt(sums[0:1, 0:1] / (3 * rank * width * tp) + SQUARE_EPS)

    outs = (c0_hbm, c1_hbm, c2_hbm)
    owns = (own01.at[0], own01.at[1], own2)
    news = (upd.at[0], upd.at[1], upd_t)
    upd_out = (u0_hbm, u1_hbm, u2_hbm)
    chunks = [(m, h) for m in range(3) for h in range(2)]

    def place(m, h, slot):
        if m < 2:
            size = block // 2
            return outs[m].at[pl.ds(pl.multiple_of(slot * block + h * size, size), size), :]
        size = width // 2
        return outs[m].at[pl.ds(h * size, size), pl.ds(pl.multiple_of(slot * block, block), block)]

    local = []
    for s in range(n_stages):
        for c, (m, h) in enumerate(chunks):
            z_first = c > 0
            if s == 0:
                size = (block if m < 2 else width) // 2
                r = pl.ds(h * size, size)
                update = scale * news[m][r, :]
                news[m][r, :] = update
                owns[m][r, :] = (wts[m][r, :] - LEARN_RATE * update).astype(BF16)
            for item in stage_items(s, z_first):
                slot, valid = item[4], item[5]
                dst = place(m, h, slot)
                src = dst
                if s > 0:
                    arrived(dst, c_recv.at[c, slot], valid)
                else:
                    size = (block if m < 2 else width) // 2
                    src = owns[m].at[pl.ds(h * size, size), :]
                forward(item, z_first, src, dst, lambda i: c_send.at[c, slot, i], c_recv.at[c, slot])
            if s == 0:
                size = (block if m < 2 else width) // 2
                r = pl.ds(h * size, size)
                local.append(pltpu.make_async_copy(owns[m].at[r, :], place(m, h, me), loc_sem.at[c]))
                local[-1].start()
                local.append(pltpu.make_async_copy(news[m].at[r, :], upd_out[m].at[r, :], loc_sem.at[6 + c]))
                local[-1].start()
    for copy in local:
        copy.wait()
    drain()


def shards(nz, nx, tp, *args):
    inputs, value_cot, gate_cot, out_cot, conv_output, factors, vw, gw, ow, m1, m2 = args
    n = nz * nx
    block, rank = factors.shape[1], factors.shape[2]
    rows, width = m1.shape[1], m1.shape[2]
    tokens = inputs.shape[0]
    features = inputs.shape[1]
    any_ = pl.BlockSpec(memory_space=pl.ANY)
    vmem = pl.BlockSpec(memory_space=pltpu.VMEM)
    dma = pltpu.SemaphoreType.DMA
    scratch = [
        pltpu.VMEM(inputs.shape, BF16),
        pltpu.VMEM(out_cot.shape, BF16),
        pltpu.VMEM((3, tokens, width), BF16),
        pltpu.VMEM((n, 3, block, rank), BF16),
        (pltpu.VMEM(vw.shape, F32), pltpu.VMEM(gw.shape, F32), pltpu.VMEM(ow.shape, F32)),
        pltpu.VMEM((3, tokens, rank), F32),
        pltpu.VMEM((n, 3, rows, width), F32),
        pltpu.VMEM((nx - 1, nz, 3, rows, width), F32),
        pltpu.VMEM((nz - 1, 3, rows, width), F32),
        pltpu.VMEM((nz, 3, rows, width), F32),
        pltpu.VMEM((n, 3, rows, width), F32),
        pltpu.VMEM((3, rank, width), BF16),
        pltpu.VMEM((3, rank, width), BF16),
        pltpu.VMEM((2, block, width), F32),
        pltpu.VMEM((width, block), F32),
        pltpu.VMEM((2, block, width), BF16),
        pltpu.VMEM((width, block), BF16),
        pltpu.VMEM((tp, 8, 128), F32),
        dma((9,)), dma((12,)),
        dma((n,)), dma((n, 4)), dma((n,)), dma((n,)), dma((n, 2)), dma((n, 2)),
        dma((nx - 1, nz)), dma((nx - 1, nz)), dma((nz - 1,)), dma((nz - 1,)),
        dma((n,)), dma((n, 4)), dma((tp - 1,)), dma((tp - 1,)),
        dma((6, n)), dma((6, n, 4)),
    ]
    shape = jax.ShapeDtypeStruct
    return pl.pallas_call(
        functools.partial(kernel, nz, nx, tp),
        out_shape=(
            shape(m1.shape, F32), shape(m2.shape, F32),
            shape(vw.shape, F32), shape(gw.shape, F32), shape(ow.shape, F32),
            shape((features, width), BF16), shape((features, width), BF16), shape((width, features), BF16),
        ),
        in_specs=[any_] * 9 + [vmem] * 2,
        out_specs=(vmem, vmem) + (any_,) * 6,
        scratch_shapes=scratch,
        compiler_params=pltpu.CompilerParams(
            collective_id=0, has_side_effects=True, vmem_limit_bytes=60 * 1024 * 1024
        ),
    )(inputs, out_cot, value_cot, gate_cot, conv_output, factors, vw, gw, ow, m1, m2)


def solution(mesh):
    fs, tp = mesh.shape["fs"], mesh.shape["tp"]
    nz = 1 << (fs.bit_length() // 2)
    nx = fs // nz
    placed = (
        P("fs", None),
        P("fs", "tp"),
        P("fs", "tp"),
        P("fs", None),
        P("fs", "tp"),
        P(None, "fs", None),
        P("fs", "tp"),
        P("fs", "tp"),
        P("tp", "fs"),
        P(None, "fs", "tp"),
        P(None, "fs", "tp"),
    )
    return jax.shard_map(
        functools.partial(shards, nz, nx, tp),
        mesh=mesh,
        in_specs=placed,
        out_specs=(
            P(None, "fs", "tp"),
            P(None, "fs", "tp"),
            P("fs", "tp"),
            P("fs", "tp"),
            P("tp", "fs"),
            P(None, "tp"),
            P(None, "tp"),
            P("tp", None),
        ),
        check_vma=False,
    )
```

time: 484 us -> 237 us (0.49)
  waiting for transfers between devices: 370 us -> 0 us
  Pallas kernels: 0 us -> 216 us
  blocking collectives: 40.8 us -> 0 us
  matrix products: 25.7 us -> 0 us
  between operations: 15.1 us -> 0.66 us
  local copies, waits for them, and re-layouts: 27.6 us -> 19.6 us
    all_gather x5 -> x0, waiting for transfers between devices: 306 us -> none  [the longest x1 104 us: shards(): pieces = lax.all_gather(factors, 'fs', axis=1, tiled=True)]
    pallas_call x0 -> x1, Pallas kernels: none -> 216 us  [shards(): pl.pallas_call(functools.partial(kernel, nz, nx, tp), out_shape=(shape(m1...]
    reduce_scatter x1 -> x0, waiting for transfers between devices: 63.7 us -> none  [shards(): lax.psum_scatter(partial_value, 'fs', scatter_dimension=0, tiled=True)]
    psum x1 -> x0, blocking collectives: 40.8 us -> none  [shards(): sum_squares = lax.psum(jnp.sum(direction * direction), ('fs', 'tp'))]
    dot_general x15 -> x0, matrix products: 25.7 us -> none  [the longest x6 8.73 us: split_product(): jnp.dot(operand, lower, preferred_element_type=jnp.float32)]
    unnamed x35 -> x14, local copies, waits for them, and re-layouts: 25.8 us -> 19.6 us
  transfers between devices with their start and end apart: 6 -> 0, of which waited for: 6 -> 0; matrix products, arithmetic and copies ran while one was open for 4% -> 0% of each run, Pallas kernels for 0% -> 0%
where the time goes in v1:
time: 237 us; the launch traced here: 236 us
  Pallas kernels  216 us (91%)
  local copies, waits for them, and re-layouts  19.6 us (8%)
    pallas_call x1, Pallas kernels, shards(): pl.pallas_call(functools.partial(kernel, nz, nx, tp), out_shape=(shape(m1...  216 us
    unnamed x14, local copies, waits for them, and re-layouts  19.6 us

profile of v1, /device:TPU:0, one launch (start us, length us, event | category | flops | bytes accessed | tf_op | source)
XLA Modules:
  0.0 236.2 jit_solution(1046071053159943533)
XLA Ops:
  0.6 215.9 %shard_map.170 = (f32[3,32,512]{2,1,0:T(8,128)}, f32[3,32,512]{2,1,0:T(8,128)}, f32[512,512]{1,0:T(8,128)}, f32[512,512]{1,0:T(8,128)}, f32[512,512]{1,0:T(8,128...) custom-call(bf16[1024,4096]{1,0:T(8,128)(2,1)} %x_hbm.1, ...), custom_call_target="tpu_custom_call" | custom-call | tf_op jit(solution)/shard_map/pallas_call | solution.py:370
  216.6 0.0 copy-start.2
  216.6 1.8 copy.27
  218.4 1.6 copy.28
  220.0 2.3 copy.29
  222.2 2.3 copy.30
  224.5 2.3 copy.31
  226.8 0.0 copy-done.2
  226.8 0.0 copy-start.1
  226.8 2.1 copy.32
  228.9 1.6 copy-done.1
  230.5 0.0 copy-start
  230.5 2.1 copy.33
  232.6 1.6 copy-done
  234.2 2.0 copy.34
Async XLA Ops:
  216.6 10.2 %copy-start.2 = (bf16[4096,512]{1,0:T(8,128)(2,1)S(1)}, bf16[4096,512]{1,0:T(8,128)(2,1)}, u32[]{:S(2)}) copy-start(bf16[4096,512]{1,0:T(8,128)(2,1)} %get-tuple-element.21) | copy-start | bytes 12582916
  226.8 3.7 %copy-start.1 = (bf16[4096,512]{1,0:T(8,128)(2,1)S(1)}, bf16[4096,512]{1,0:T(8,128)(2,1)}, u32[]{:S(2)}) copy-start(bf16[4096,512]{1,0:T(8,128)(2,1)} %get-tuple-element.22) | copy-start | bytes 12582916
  230.5 3.7 %copy-start = (bf16[512,4096]{1,0:T(8,128)(2,1)S(1)}, bf16[512,4096]{1,0:T(8,128)(2,1)}, u32[]{:S(2)}) copy-start(bf16[512,4096]{1,0:T(8,128)(2,1)} %get-tuple-element.23) | copy-start | bytes 12582916

commit v2 on v1

v2 whole, which is shorter than its diff:
```python
import functools

import jax
import jax.numpy as jnp
from jax import lax
from jax.experimental import pallas as pl
from jax.experimental.pallas import tpu as pltpu
from jax.sharding import PartitionSpec as P

FIRST_DECAY = 0.9
SECOND_DECAY = 0.95
DIVISOR_EPS = 1e-08
SQUARE_EPS = 1e-06
LEARN_RATE = 0.01
HOP, SKEW, SKEW2, RS_X, RS_Z, HOP_D = 4.2, 1.8, 3.0, 8.0, 6.0, 3.7
VMEM_BYTES = 45 * 1024 * 1024
MESH = pl.DeviceIdType.MESH
F32 = jnp.float32
BF16 = jnp.bfloat16


def high_low(values):
    upper = values.astype(BF16)
    lower = (values - upper.astype(F32)).astype(BF16)
    return upper, lower


def others(coord, size, dist):
    if dist == 0:
        return [(coord, 0, None)]
    if size == 2:
        return [(1 - coord, None, None)]
    return [(coord - dist, -1, coord >= dist), (coord + dist, 1, coord + dist < size)]


def both(*preds):
    preds = [p for p in preds if p is not None]
    if not preds:
        return None
    return functools.reduce(jnp.logical_and, preds)


def run_if(pred, fn):
    if pred is None:
        fn()
    else:
        pl.when(pred)(fn)


def kernel(
    nz, nx, tp,
    x_hbm, oc_hbm, vc_hbm, gc_hbm, co_hbm, f_hbm, w0_hbm, w1_hbm, w2_hbm, m1_ref, m2_ref,
    nf_ref, ns_ref, u0_ref, u1_ref, u2_ref, c0_ref, c1_ref, c2_ref,
    x_v, oc_v, cots, fg, wts, acc, part, rx, rz, q, dg, dh, dl, ss,
    in_sem, f_recv, f_send, y_recv, y_send, p_recv, p_send,
    rx_recv, rx_send, rz_recv, rz_send, d_recv, d_send, s_recv, s_send, c_recv, c_send,
):
    me = lax.axis_index("fs")
    t = lax.axis_index("tp")
    z = lax.div(me, nx)
    x = lax.rem(me, nx)
    n = nz * nx
    core = lax.rem(t, 2)
    row = lax.rem(lax.div(t, 2), 2)
    mate = t + 1 - 2 * core
    beside = t + 2 - 4 * row
    block = f_hbm.shape[1]
    rank = f_hbm.shape[2]
    rows = m1_ref.shape[1]
    width = m1_ref.shape[2]
    tokens = x_hbm.shape[0]
    pending = []

    def remote(src, dst, ssem, rsem, where):
        copy = pltpu.make_async_remote_copy(
            src_ref=src, dst_ref=dst, send_sem=ssem, recv_sem=rsem,
            device_id=where, device_id_type=MESH,
        )
        return copy

    def send(src, dst, ssem, rsem, where, pred, outer):
        copy = remote(src, dst, ssem, rsem, where)
        pred = both(pred, outer)
        run_if(pred, copy.start)
        pending.append((pred, copy))

    def drain():
        for pred, copy in pending:
            run_if(pred, copy.wait_send)
        pending.clear()

    loads = [
        pltpu.make_async_copy(f_hbm, fg.at[:, me], in_sem.at[0]),
        pltpu.make_async_copy(x_hbm, x_v, in_sem.at[1]),
        pltpu.make_async_copy(oc_hbm, oc_v, in_sem.at[2]),
        pltpu.make_async_copy(vc_hbm, cots.at[0], in_sem.at[3]),
        pltpu.make_async_copy(gc_hbm, cots.at[1], in_sem.at[4]),
        pltpu.make_async_copy(co_hbm, cots.at[2], in_sem.at[5]),
        pltpu.make_async_copy(w0_hbm, wts[0], in_sem.at[6]),
        pltpu.make_async_copy(w1_hbm, wts[1], in_sem.at[7]),
        pltpu.make_async_copy(w2_hbm, wts[2], in_sem.at[8]),
    ]
    for load in loads:
        load.start()

    barrier = pltpu.get_barrier_semaphore()
    peers = [{"fs": lax.rem(z + k, nz) * nx + x} for k in range(1, nz)]
    peers += [{"fs": z * nx + lax.rem(x + k, nx)} for k in range(1, nx)]
    peers += [{"tp": lax.rem(t + k, tp)} for k in range(1, tp)]
    for peer in peers:
        pl.semaphore_signal(barrier, inc=1, device_id=peer, device_id_type=MESH)
    pl.semaphore_wait(barrier, len(peers))

    def stage_items(s, z_first):
        n1, n2 = (nz, nx) if z_first else (nx, nz)
        c1, c2 = (z, x) if z_first else (x, z)
        items = []
        for e in range(0, n2):
            d = s - e
            if d < 0 or d >= n1:
                continue
            for o1, s1, v1 in others(c1, n1, d):
                for o2, s2, v2 in others(c2, n2, e):
                    slot = o1 * nx + o2 if z_first else o2 * nx + o1
                    items.append((d, e, s1, s2, slot, both(v1, v2)))
        return items

    def forward(item, z_first, src, dst, ssem, rsem):
        d, e, s1, s2, slot, valid = item
        n1, n2 = (nz, nx) if z_first else (nx, nz)
        c1, c2 = (z, x) if z_first else (x, z)
        st1, st2 = (nx, 1) if z_first else (1, nx)
        if e == 0:
            if s1 in (-1, 0):
                send(src, dst, ssem(0), rsem, {"fs": me + st1}, c1 + 1 < n1, valid)
            if s1 in (1, 0):
                send(src, dst, ssem(1 if s1 == 0 else 0), rsem, {"fs": me - st1}, c1 > 0, valid)
        if s2 in (-1, 0):
            send(src, dst, ssem(2), rsem, {"fs": me + st2}, c2 + 1 < n2, valid)
        if s2 in (1, 0):
            send(src, dst, ssem(3 if s2 == 0 else 2), rsem, {"fs": me - st2}, c2 > 0, valid)

    def arrived(dst, sem, pred=None):
        run_if(pred, pltpu.make_async_copy(dst, dst, sem).wait)

    unit = block // 16
    half = core * (block // 2)
    fs_start = pl.multiple_of(half + row * 3 * unit, unit)
    y_send_start = pl.multiple_of(half + row * 5 * unit, unit)
    y_recv_start = pl.multiple_of(half + (1 - row) * 5 * unit, unit)
    mate_half = (1 - core) * (block // 2)
    mate_fs_start = pl.multiple_of(mate_half + row * 3 * unit, unit)
    mate_y_start = pl.multiple_of(mate_half + (1 - row) * 5 * unit, unit)

    def f_part(k, slot, start, units):
        return fg.at[k, slot, pl.ds(start, units * unit), :]

    sources = (x_v, x_v, oc_v)

    def matmul(k, slot, first):
        cols = pl.ds(pl.multiple_of(slot * block, block), block)
        tile = 256

        def body(i, carry):
            r = pl.ds(pl.multiple_of(i * tile, tile), tile)
            prod = jnp.dot(sources[k][r, cols], fg[k, slot], preferred_element_type=F32)
            if first:
                acc[k, r, :] = prod
            else:
                acc[k, r, :] += prod
            return carry

        lax.fori_loop(0, tokens // tile, body, 0)

    n_stages = nz + nx - 1
    stages = [stage_items(s, True) for s in range(n_stages)]

    def f_arrive(k, s):
        for item in stages[s]:
            slot, valid = item[4], item[5]
            piece = f_part(k, slot, fs_start, 5)
            if s > 0:
                arrived(piece, f_recv.at[k, slot], valid)
            forward(item, True, piece, piece, lambda i: f_send.at[k, slot, i], f_recv.at[k, slot])
            if s > 0:
                ypiece = f_part(k, slot, y_send_start, 3)
                send(ypiece, ypiece, y_send.at[k, slot], y_recv.at[k, slot], {"tp": beside}, None, valid)
                send(piece, piece, p_send.at[k, slot, 0], p_recv.at[k, slot, 0], {"tp": mate}, None, valid)

    def f_pass(k, s):
        for item in stages[s]:
            slot, valid = item[4], item[5]
            ypiece = f_part(k, slot, y_recv_start, 3)
            arrived(ypiece, y_recv.at[k, slot], valid)
            send(ypiece, ypiece, p_send.at[k, slot, 1], p_recv.at[k, slot, 1], {"tp": mate}, None, valid)

    def f_use(k, s):
        for item in stages[s]:
            slot, valid = item[4], item[5]

            def use(slot=slot):
                arrived(f_part(k, slot, mate_fs_start, 5), p_recv.at[k, slot, 0])
                arrived(f_part(k, slot, mate_y_start, 3), p_recv.at[k, slot, 1])
                matmul(k, slot, False)

            run_if(valid, use)

    dims = (((0,), (0,)), ((), ()))
    order = list(range(1, nz)) + [0]

    def partial(k):
        loads[3 + k].wait()
        upper, lower = high_low(acc[k])
        prod = lax.dot_general(upper, cots[k], dims, preferred_element_type=F32)
        prod = prod + lax.dot_general(lower, cots[k], dims, preferred_element_type=F32)
        part[k] = prod.reshape(n, rows, width)
        for i in order:
            oz = lax.rem(z + i, nz)
            for e in range(1, nx):
                slot = oz * nx + lax.rem(x + e, nx)
                send(
                    part.at[k, slot], rx.at[k, e - 1, i], rx_send.at[k, e - 1, i], rx_recv.at[k, e - 1, i],
                    {"fs": z * nx + lax.rem(x + e, nx)}, None, None,
                )

    def along_z(k):
        for i in order:
            oz = lax.rem(z + i, nz)
            value = part[k, oz * nx + x]
            for e in range(1, nx):
                arrived(rx.at[k, e - 1, i], rx_recv.at[k, e - 1, i])
                value = value + rx[k, e - 1, i]
            q[k, i] = value
            if i:
                send(
                    q.at[k, i], rz.at[k, i - 1], rz_send.at[k, i - 1], rz_recv.at[k, i - 1],
                    {"fs": oz * nx + x}, None, None,
                )

    def moments(k):
        projected = q[k, 0]
        for i in range(1, nz):
            arrived(rz.at[k, i - 1], rz_recv.at[k, i - 1])
            projected = projected + rz[k, i - 1]
        new_first = FIRST_DECAY * m1_ref[k] + (1.0 - FIRST_DECAY) * projected
        new_second = SECOND_DECAY * m2_ref[k] + (1.0 - SECOND_DECAY) * projected * projected
        nf_ref[k] = new_first
        ns_ref[k] = new_second
        dg[k, me] = new_first / (jnp.sqrt(new_second) + DIVISOR_EPS)
        d_arrive(k, 0)

    def d_arrive(k, s):
        for item in stages[s]:
            slot, valid = item[4], item[5]
            piece = dg.at[k, slot]
            if s > 0:
                arrived(piece, d_recv.at[k, slot], valid)
            forward(item, True, piece, piece, lambda i: d_send.at[k, slot, i], d_recv.at[k, slot])

    tdims = (((0,), (1,)), ((), ()))
    news = (u0_ref, u1_ref, u2_ref)

    def unscaled(k):
        value = dg[k].reshape(rank, width)
        upper, lower = high_low(value)
        dh[k] = upper
        dl[k] = lower
        if k < 2:
            news[k][...] = jnp.dot(fg[k, me], dh[k], preferred_element_type=F32) + jnp.dot(
                fg[k, me], dl[k], preferred_element_type=F32
            )
        else:
            news[k][...] = lax.dot_general(dh[k], fg[k, me], tdims, preferred_element_type=F32) + lax.dot_general(
                dl[k], fg[k, me], tdims, preferred_element_type=F32
            )

    def squares(k):
        value = dg[k].reshape(rank, width)
        return jnp.sum(value * value, axis=0, keepdims=True)

    loads[0].wait()
    for k in range(3):
        f_arrive(k, 0)

    def own_part(k):
        if k != 1:
            loads[1 + k // 2].wait()
        matmul(k, me, True)

    steps = []
    hop, skew = HOP, SKEW
    for k in range(3):
        for s in range(1, n_stages):
            at = s * hop + k * skew
            steps.append((at, 0, k, s, f_arrive))
            steps.append((at + 3.5, 1, k, s, f_pass))
            steps.append((at + 6.0, 2, k, s, f_use))
        steps.append((8.5 + 0.5 * k, 2, k, None, own_part))
        at = (n_stages - 1) * hop + 8.0 + k * SKEW2
        steps.append((at, 3, k, None, partial))
        steps.append((at + RS_X, 4, k, None, along_z))
        at = at + RS_X + RS_Z
        steps.append((at, 5, k, None, moments))
        for s in range(1, n_stages):
            steps.append((at + s * HOP_D, 6, k, s, d_arrive))
    steps.sort(key=lambda step: step[:3])
    for _, _, k, s, step in steps:
        if s is None:
            step(k)
        else:
            step(k, s)
    unscaled(0)
    total = squares(0)
    total = jnp.sum(total + squares(1) + squares(2), axis=1, keepdims=True)
    ss[0] = jnp.broadcast_to(total, ss.shape[1:])
    for j in range(1, tp):
        send(ss.at[0], ss.at[j], s_send.at[j - 1], s_recv.at[j - 1], {"tp": lax.rem(t + j, tp)}, None, None)
    unscaled(1)
    unscaled(2)
    for load in loads[6:9]:
        load.wait()
    sums = ss[0]
    for j in range(1, tp):
        arrived(ss.at[j], s_recv.at[j - 1])
        sums = sums + ss[j]
    scale = lax.rsqrt(sums[0:1, 0:1] / (3 * rank * width * tp) + SQUARE_EPS)

    outs = (c0_ref, c1_ref, c2_ref)
    chunks = [(m, h) for m in range(3) for h in range(2)]

    def place(m, h, slot):
        if m < 2:
            size = block // 2
            return outs[m].at[pl.ds(pl.multiple_of(slot * block + h * size, size), size), :]
        size = width // 2
        return outs[m].at[pl.ds(h * size, size), pl.ds(pl.multiple_of(slot * block, block), block)]

    for s in range(n_stages):
        for c, (m, h) in enumerate(chunks):
            z_first = c > 0
            if s == 0:
                size = (block if m < 2 else width) // 2
                r = pl.ds(h * size, size)
                update = scale * news[m][r, :]
                news[m][r, :] = update
                place(m, h, me)[...] = (wts[m][r, :] - LEARN_RATE * update).astype(BF16)
            for item in stage_items(s, z_first):
                slot, valid = item[4], item[5]
                dst = place(m, h, slot)
                if s > 0:
                    arrived(dst, c_recv.at[c, slot], valid)
                forward(item, z_first, dst, dst, lambda i: c_send.at[c, slot, i], c_recv.at[c, slot])
    drain()


def store_kernel(*refs):
    count = (len(refs) - 1) // 2
    sems = refs[-1]
    copies = [pltpu.make_async_copy(refs[i], refs[count + i], sems.at[i]) for i in range(count)]
    for copy in copies:
        copy.start()
    for copy in copies:
        copy.wait()


def shards(nz, nx, tp, *args):
    inputs, value_cot, gate_cot, out_cot, conv_output, factors, vw, gw, ow, m1, m2 = args
    n = nz * nx
    block, rank = factors.shape[1], factors.shape[2]
    rows, width = m1.shape[1], m1.shape[2]
    tokens = inputs.shape[0]
    features = inputs.shape[1]
    any_ = pl.BlockSpec(memory_space=pl.ANY)
    vmem = pl.BlockSpec(memory_space=pltpu.VMEM)
    dma = pltpu.SemaphoreType.DMA
    scratch = [
        pltpu.VMEM(inputs.shape, BF16),
        pltpu.VMEM(out_cot.shape, BF16),
        pltpu.VMEM((3, tokens, width), BF16),
        pltpu.VMEM((3, n, block, rank), BF16),
        (pltpu.VMEM(vw.shape, F32), pltpu.VMEM(gw.shape, F32), pltpu.VMEM(ow.shape, F32)),
        pltpu.VMEM((3, tokens, rank), F32),
        pltpu.VMEM((3, n, rows, width), F32),
        pltpu.VMEM((3, nx - 1, nz, rows, width), F32),
        pltpu.VMEM((3, nz - 1, rows, width), F32),
        pltpu.VMEM((3, nz, rows, width), F32),
        pltpu.VMEM((3, n, rows, width), F32),
        pltpu.VMEM((3, rank, width), BF16),
        pltpu.VMEM((3, rank, width), BF16),
        pltpu.VMEM((tp, 8, 128), F32),
        dma((9,)),
        dma((3, n)), dma((3, n, 4)), dma((3, n)), dma((3, n)), dma((3, n, 2)), dma((3, n, 2)),
        dma((3, nx - 1, nz)), dma((3, nx - 1, nz)), dma((3, nz - 1)), dma((3, nz - 1)),
        dma((3, n)), dma((3, n, 4)), dma((tp - 1,)), dma((tp - 1,)),
        dma((6, n)), dma((6, n, 4)),
    ]
    shape = [
        (m1.shape, F32), (m2.shape, F32), (vw.shape, F32), (gw.shape, F32), (ow.shape, F32),
        ((features, width), BF16), ((features, width), BF16), ((width, features), BF16),
    ]
    held = pl.pallas_call(
        functools.partial(kernel, nz, nx, tp),
        out_shape=tuple(pltpu.VMEM(*item) for item in shape),
        in_specs=[any_] * 9 + [vmem] * 2,
        out_specs=(vmem,) * 8,
        scratch_shapes=scratch,
        compiler_params=pltpu.CompilerParams(
            collective_id=0, has_side_effects=True, vmem_limit_bytes=VMEM_BYTES
        ),
    )(inputs, out_cot, value_cot, gate_cot, conv_output, factors, vw, gw, ow, m1, m2)
    return pl.pallas_call(
        store_kernel,
        out_shape=tuple(jax.ShapeDtypeStruct(*item) for item in shape),
        in_specs=[vmem] * 8,
        out_specs=(any_,) * 8,
        scratch_shapes=[dma((8,))],
        compiler_params=pltpu.CompilerParams(vmem_limit_bytes=1024 * 1024),
    )(*held)


def solution(mesh):
    fs, tp = mesh.shape["fs"], mesh.shape["tp"]
    nz = 1 << (fs.bit_length() // 2)
    nx = fs // nz
    placed = (
        P("fs", None),
        P("fs", "tp"),
        P("fs", "tp"),
        P("fs", None),
        P("fs", "tp"),
        P(None, "fs", None),
        P("fs", "tp"),
        P("fs", "tp"),
        P("tp", "fs"),
        P(None, "fs", "tp"),
        P(None, "fs", "tp"),
    )
    return jax.shard_map(
        functools.partial(shards, nz, nx, tp),
        mesh=mesh,
        in_specs=placed,
        out_specs=(
            P(None, "fs", "tp"),
            P(None, "fs", "tp"),
            P("fs", "tp"),
            P("fs", "tp"),
            P("tp", "fs"),
            P(None, "tp"),
            P(None, "tp"),
            P("tp", None),
        ),
        check_vma=False,
    )
```

time: 237 us -> 220 us (0.928)
  local copies, waits for them, and re-layouts: 19.6 us -> 0 us
  Pallas kernels: 216 us -> 219 us
    unnamed x14 -> x0, local copies, waits for them, and re-layouts: 19.6 us -> none
    pallas_call x1 -> x2, Pallas kernels: 216 us -> 219 us  [the longest x1 213 us: shards(): pl.pallas_call(functools.partial(kernel, nz, nx, tp), out_shape=tuple((pl...]
where the time goes in v2:
time: 220 us
  Pallas kernels  219 us (100%)
    pallas_call x1, Pallas kernels, shards(): pl.pallas_call(functools.partial(kernel, nz, nx, tp), out_shape=tuple((pl...  213 us
    pallas_call x1, Pallas kernels, shards(): pl.pallas_call(store_kernel, out_shape=tuple((jax.ShapeDtypeStruct(*item)...  5.89 us

profile of v2, /device:TPU:0, one launch (start us, length us, event | category | flops | bytes accessed | tf_op | source)
XLA Modules:
  0.0 220.0 jit_solution(4021653694185188818)
XLA Ops:
  0.6 213.3 %shard_map.170 = (f32[3,32,512]{2,1,0:T(8,128)S(1)}, f32[3,32,512]{2,1,0:T(8,128)S(1)}, f32[512,512]{1,0:T(8,128)S(1)}, f32[512,512]{1,0:T(8,128)S(1)}, f32[512,...) custom-call(bf16[1024,4096]{1,0:T(8,128)(2,1)} %x_hbm.1, ...), custom_call_target="tpu_custom_call" | custom-call | tf_op jit(solution)/shard_map/pallas_call | solution.py:401
  214.0 5.9 %shard_map.171 = (f32[3,32,512]{2,1,0:T(8,128)}, f32[3,32,512]{2,1,0:T(8,128)}, f32[512,512]{1,0:T(8,128)}, f32[512,512]{1,0:T(8,128)}, f32[512,512]{1,0:T(8,128...) custom-call(f32[3,32,512]{2,1,0:T(8,128)S(1)} %get-tuple-element.16.refs_0_, ...), custom_call_target="tpu_custom_call" | custom-call | tf_op jit(solution)/shard_map/pallas_call | solution.py:411
